TPU v7x, 256 devices: a whole 4x4x8 slice. The times are simulated.
256 devices in a mesh: gr: 2 (over z_hi), fs: 16 (over z_lo, y), tp: 8 (over x, core).
Axes of the slice: x: 4, y: 4, z: 8 (z_hi: 2, z_lo: 4; z = z_hi * 4 + z_lo), core: 2. Of those that a mesh axis runs over, the one named last changes fastest.
Arguments:
- tokens: bfloat16 [8192, 2048], P(('gr', 'fs')), may hold values from -6 to 6
- route_ids: int32 [8192, 4], P(('gr', 'fs')), may hold values from 0 to 15, all different within a row; in each aligned block of 256 rows (0 to 255, 256 to 511, ...) at most 80 rows name the same one
- route_scores: float32 [8192, 4], P(('gr', 'fs')), may hold values from -4 to 4
- norm_gain: float32 [2048], P(('gr', 'fs')), may hold values from 0.1 to 1.9
- gate_weight: float32 [16, 2048, 2048], P(None, ('gr', 'fs'), 'tp'), may hold values from -0.5 to 0.5
- up_weight: float32 [16, 2048, 2048], P(None, ('gr', 'fs'), 'tp'), may hold values from -0.5 to 0.5
- down_weight: float32 [16, 2048, 2048], P(None, ('gr', 'fs'), 'tp'), may hold values from -0.03125 to 0.03125
Outputs:
- served_gate: bfloat16 [16, 2048, 2048], P('fs', None, 'tp')
- served_up: bfloat16 [16, 2048, 2048], P('fs', None, 'tp')
- served_down: bfloat16 [16, 2048, 2048], P('fs', None, 'tp')
- expert_mix: bfloat16 [8192, 2048], P(('gr', 'fs'), 'tp')
Inputs may be any that keep to these rules, and one draw needn't show every extreme that they name: `route_ids`: in each aligned block of 256 rows no expert is named by more than 80 pairs, and in some blocks one expert is named by exactly 80. The 4 experts of a token differ.
All inputs are finite; a program needn't handle non-finite values.
Results may differ from a plain program's by a relative error of at most 0.0092.
Values may be sent and summed in bfloat16 or wider, within the bound.
A program may use at most 64 MiB of HBM per device.

v0:
```python
import jax
import jax.numpy as jnp
from jax import lax
from jax.sharding import PartitionSpec as P

EXPERTS = 16
CAP = 80
norm_eps = 1e-06
clamp_limit = 7.0
sigmoid_slope = 1.702


def sent_together(arrays, axis, split_dim, concat_dim, along):
    ends, at = ([], 0)
    for a in arrays[:-1]:
        at += a.shape[along]
        ends.append(at)
    both = jnp.concatenate(arrays, axis=along)
    return tuple(
        jnp.split(
            lax.all_to_all(both, axis, split_axis=split_dim, concat_axis=concat_dim, tiled=True),
            ends,
            axis=along,
        )
    )


def laid_out(parts, dim):
    lengths = list(parts.shape[1:])
    lengths[dim] *= parts.shape[0]
    return jnp.moveaxis(parts, 0, dim).reshape(lengths)


def from_everyone(array, axis):
    devices = lax.axis_size(axis)
    return lax.all_to_all(
        jnp.broadcast_to(array[None], (devices, *array.shape)), axis, 0, 0, tiled=True
    )


def gathered_copies(array, axis, dim):
    return laid_out(from_everyone(array, axis), dim)


def side_by_side(arrays, axis, dim, along):
    widths = [a.shape[along] for a in arrays]
    both = jnp.concatenate(arrays, axis=along)
    filled = gathered_copies(both, axis, dim)
    return tuple(jnp.split(filled, [sum(widths[:k]) for k in range(1, len(widths))], axis=along))


def route_tables(block_ids, block_scores):
    row_count, top_count = block_ids.shape
    flattened = block_ids.reshape(-1)
    onehot = (flattened[:, None] == jnp.arange(EXPERTS, dtype=jnp.int32)[None, :]).astype(jnp.int32)
    before = jnp.cumsum(onehot, axis=0) - onehot
    slot_index = jnp.sum(before * onehot, axis=1)
    target = flattened * CAP + slot_index
    matches = (target[:, None] == jnp.arange(EXPERTS * CAP, dtype=jnp.int32)[None, :]).astype(
        jnp.float32
    )
    matches = matches.reshape(row_count, top_count, EXPERTS * CAP)
    exponent = jnp.exp(block_scores)
    weights = (exponent / jnp.sum(exponent, axis=1, keepdims=True)).astype(jnp.bfloat16)
    dispatch = jnp.sum(matches, axis=1).T.astype(jnp.bfloat16)
    combine = jnp.einsum("tk,tkc->tc", weights.astype(jnp.float32), matches).astype(jnp.bfloat16)
    return (dispatch, combine)


def activate(gate_pre, up_pre):
    clipped_gate = jnp.minimum(gate_pre, clamp_limit)
    clipped_up = jnp.clip(up_pre, -clamp_limit, clamp_limit)
    return (
        clipped_gate * jax.nn.sigmoid(sigmoid_slope * clipped_gate) * (clipped_up + 1.0)
    ).astype(jnp.bfloat16)


def local(tokens, route_ids, route_scores, norm_gain, gate_weight, up_weight, down_weight):
    scaling = norm_gain[None, :, None]
    folded = (
        (scaling * gate_weight).astype(jnp.bfloat16),
        (scaling * up_weight).astype(jnp.bfloat16),
        down_weight.astype(jnp.bfloat16),
    )
    by_expert = sent_together((folded[0], folded[1], folded[2]), "fs", 0, 1, 2)
    served_gate, served_up, served_down = side_by_side(
        (by_expert[0], by_expert[1], by_expert[2]), "gr", 1, 0
    )
    as_float = tokens.astype(jnp.float32)
    normed = (
        as_float * lax.rsqrt(jnp.mean(as_float * as_float, axis=1, keepdims=True) + norm_eps)
    ).astype(jnp.bfloat16)
    dispatch, combine = route_tables(route_ids, route_scores)
    column_width = normed.shape[1] // lax.axis_size("tp")
    normed = lax.dynamic_slice_in_dim(normed, lax.axis_index("tp") * column_width, column_width, 1)
    slot_rows = jnp.dot(dispatch, normed, preferred_element_type=jnp.float32).astype(jnp.bfloat16)
    outgoing = slot_rows.reshape(EXPERTS, 1, CAP, slot_rows.shape[1])
    portion = lax.all_gather(
        lax.all_to_all(outgoing, "fs", split_axis=0, concat_axis=1, tiled=True),
        "tp",
        axis=3,
        tiled=True,
    )
    gate_pre = jnp.einsum(
        "egnd,edf->egnf", portion, served_gate, preferred_element_type=jnp.float32
    )
    up_pre = jnp.einsum("egnd,edf->egnf", portion, served_up, preferred_element_type=jnp.float32)
    hidden = activate(gate_pre, up_pre)
    summed = jnp.einsum(
        "egnf,efd->egnd",
        lax.all_gather(hidden, "tp", axis=3, tiled=True),
        served_down,
        preferred_element_type=jnp.float32,
    )
    results = summed.astype(jnp.bfloat16)
    returned = lax.all_to_all(results, "fs", split_axis=1, concat_axis=0, tiled=True)
    flattened = returned.reshape(EXPERTS * CAP, returned.shape[3])
    expert_mix = jnp.dot(combine, flattened, preferred_element_type=jnp.float32).astype(
        jnp.bfloat16
    )
    return (served_gate, served_up, served_down, expert_mix)


def solution(mesh):
    in_specs = (
        P(("gr", "fs"), None),
        P(("gr", "fs"), None),
        P(("gr", "fs"), None),
        P(("gr", "fs")),
        P(None, ("gr", "fs"), "tp"),
        P(None, ("gr", "fs"), "tp"),
        P(None, ("gr", "fs"), "tp"),
    )
    out_specs = (
        P("fs", None, "tp"),
        P("fs", None, "tp"),
        P("fs", None, "tp"),
        P(("gr", "fs"), "tp"),
    )
    return jax.shard_map(local, mesh=mesh, in_specs=in_specs, out_specs=out_specs, check_vma=False)
```

profile of v0, /device:TPU:32, one launch (start us, length us, event | category | flops | bytes accessed | tf_op | source)
XLA Modules:
  0.0 250.1 jit_solution(6966143844637540849)
XLA Ops:
  7.2 0.0 all-gather.5.cloned.1.call-start
  7.2 0.8 copy.39
  8.0 0.1 eq.44
  8.2 0.1 eq.40
  8.3 0.0 copy-start
  8.3 1.5 convert_element_type.64
  9.8 0.0 copy-done
  9.9 0.0 copy-start.7
  9.9 0.3 multiply_reduce_fusion
  10.2 4.5 %reduce-window.6 = s32[16,8,128]{2,1,0:T(8,128)S(1)} reduce-window(s32[16,8,128]{2,1,0:T(8,128)S(1)} %fusion.29, s32[]{:T(128)} %constant.14.clone.1), window={size=1x1x128 pad=0_0x0_0x127_0}, to_apply=%region_1.0 | reduce-window | flops 2080768 | bytes 131076 | tf_op jit(solution)/shard_map/reduce-window
  14.7 0.1 slice.11
  14.8 0.1 copy.41
  14.9 0.1 copy.42
  15.0 0.1 broadcast_add_fusion
  15.1 0.1 reduce_sum.40
  15.3 0.1 copy.43
  15.3 0.0 copy-done.7
  15.4 0.8 convert_reduce_fusion
  16.2 0.4 convolution_convert_fusion
  16.6 0.0 copy-start.1
  16.6 0.0 copy-start.2
  16.6 0.0 copy-start.3
  16.6 0.0 copy-start.9
  16.7 26.7 %all_to_all.38 = bf16[16,1,80,256]{3,2,1,0:T(8,128)(2,1)} all-to-all(bf16[16,1,80,256]{3,2,1,0:T(8,128)(2,1)S(1)} %bitcast.70), channel_id=1, replica_groups=mesh['gr'=2,'fs'=16,'tp'=8] {'fs'}, dimensions={0} | all-to-all | bytes 1310720 | tf_op jit(solution)/shard_map/all_to_all | solution.py:99
  43.4 0.0 all-gather.5.cloned.1.call-update
  43.4 0.0 all-gather.7.cloned.1.call-start
  43.4 0.0 copy-done.1
  43.4 0.1 convert_element_type.57
  43.5 0.0 copy-done.2
  43.5 0.0 copy-done.3
  43.5 0.0 copy-done.9
  43.5 0.3 multiply_convert_fusion.1
  43.9 0.1 pad_maximum_fusion
  44.0 41.9 %all_to_all.39 = bf16[16,64,768]{2,1,0:T(8,128)(2,1)S(1)} all-to-all(bf16[16,64,768]{2,1,0:T(8,128)(2,1)S(1)} %pad_maximum_fusion), channel_id=1, replica_groups=mesh['gr'=2,'fs'=16,'tp'=8] {'fs'}, dimensions={0} | all-to-all | bytes 3145728 | tf_op jit(solution)/shard_map/all_to_all | solution.py:21
  85.9 0.1 fusion.33
  86.0 0.2 pad_maximum_fusion.1
  86.1 0.2 broadcast_in_dim.2
  86.4 77.5 %all_to_all.40 = bf16[2,3,1024,256]{3,2,1,0:T(8,128)(2,1)S(1)} all-to-all(bf16[2,3,1024,256]{3,2,1,0:T(8,128)(2,1)S(1)} %broadcast_in_dim.2), channel_id=1, replica_groups=mesh['gr'=2,'fs'=16,'tp'=8] {'gr'}, dimensions={0} | all-to-all | bytes 6291456 | tf_op jit(solution)/shard_map/all_to_all | solution.py:36
  163.8 0.2 fusion.32
  164.1 0.0 copy-start.6
  164.1 0.0 copy-start.5
  164.1 0.0 copy-start.4
  164.1 0.0 all-gather.5.cloned.1.call-done
  164.1 0.0 copy-start.10
  164.1 5.2 %fusion.9 = f32[16,80,256]{2,1,0:T(8,128)S(1)} fusion(bf16[2048,256,1]{1,0,2:T(8,128)(2,1)S(1)} %bitcast.76, bf16[16,1,80,2048]{3,2,0,1:T(8,128)(2,1)} %all-gather.5.cloned.1.call-done), kind=kOutput, calls=%fused_computation.13 | convolution fusion | flops 1342504960 | bytes 7602176 | tf_op jit(solution)/shard_map/egnd,edf->egnf/dot_general | solution.py:104
  169.3 0.0 copy-done.6
  169.3 0.0 copy-done.5
  169.3 0.0 copy-done.10
  169.3 2.7 %fusion.18 = bf16[16,80,256]{2,1,0:T(8,128)(2,1)} fusion(bf16[2048,256,1]{1,0,2:T(8,128)(2,1)S(1)} %bitcast.74, bf16[16,1,80,2048]{3,2,0,1:T(8,128)(2,1)S(1)} %copy-done.10, f32[16,80,256]{2,1,0:T(8,128)S(1)} %fusion.9), kind=kOutput, calls=%fused_computation.16 | convolution fusion | flops 1345126400 | bytes 8257536 | tf_op jit(solution)/shard_map/egnd,edf->egnf/dot_general | solution.py:107
  172.0 0.0 all-gather.7.cloned.1.call-update
  172.1 39.6 %all-gather.7.cloned.1.call-done = bf16[16,80,2048]{2,1,0:T(8,128)(2,1)} async-done(((bf16[16,80,256]{2,1,0:T(8,128)(2,1)}), bf16[16,80,2048]{2,1,0:T(8,128)(2,1)}) %all-gather.7.cloned.1.call-update) | async-done | bytes 5242896 | tf_op jit(solution)/shard_map/all_gather | solution.py:111
  211.7 0.0 copy-done.4
  211.7 0.0 copy-start.8
  211.7 4.9 %fusion.21 = bf16[1,16,80,256]{3,2,0,1:T(8,128)(2,1)} fusion(bf16[16,80,2048]{2,1,0:T(8,128)(2,1)} %all-gather.7.cloned.1.call-done, bf16[2048,256,1]{1,0,2:T(8,128)(2,1)S(1)} %bitcast.72), kind=kOutput, calls=%fused_computation.19 | convolution fusion | flops 1342504960 | bytes 6946816 | tf_op jit(solution)/shard_map/egnf,efd->egnd/dot_general | solution.py:109
  216.6 7.7 %all-to-all-start.3 = ((bf16[1,16,80,256]{3,2,0,1:T(8,128)(2,1)}), bf16[1,16,80,256]{3,2,0,1:T(8,128)(2,1)S(1)}, u32[]{:S(2)}, u32[]{:S(2)}) async-start(bf16[1,16,80,256]{3,2,0,1:T(8,128)(2,1)} %fusion.21), calls=%async_computation.3 | async-start | bytes 1310720 | tf_op jit(solution)/shard_map/all_to_all | solution.py:116
  224.4 0.0 copy-done.8
  224.4 0.2 copy.47
  224.6 0.8 iota_compare_fusion
  225.4 3.4 %fusion.4 = bf16[256,1,1280]{2,1,0:T(2,128)(2,1)S(1)} fusion(bf16[256,4,1]{1,2,0:T(2,128)(2,1)S(1)} %copy.47, pred[256,4,1280]{2,0,1:T(32,128)(4,1)S(1)} %iota_compare_fusion), kind=kOutput, calls=%fused_computation.6 | convolution fusion | flops 2621440 | bytes 1968128 | tf_op jit(solution)/shard_map/tk,tkc->tc/dot_general | solution.py:66
  228.8 13.5 %all-to-all-done.3 = bf16[1,16,80,256]{3,2,0,1:T(8,128)(2,1)S(1)} async-done(((bf16[1,16,80,256]{3,2,0,1:T(8,128)(2,1)}), bf16[1,16,80,256]{3,2,0,1:T(8,128)(2,1)S(1)}, u32[]{:S(2)}, u32[]{:S(2)}) %all-to-all-start.3) | async-done | bytes 655392 | tf_op jit(solution)/shard_map/all_to_all | solution.py:116
  242.3 1.0 convolution_convert_fusion.2
  (8 shorter events, 0.1 us)
Async XLA Ops:
  7.2 157.0 %all-gather.5.cloned.1.call-start = ((), (), s32[]{:S(2)}) async-start(), calls=%async_computation.4 | async-start | bytes 5898240 | tf_op jit(solution)/shard_map/all_gather | solution.py:98
  8.3 1.6 copy-start
  9.9 5.5 %copy-start.7 = (s32[256,4]{0,1:T(4,128)S(1)}, s32[256,4]{0,1:T(4,128)}, u32[]{:S(2)}) copy-start(s32[256,4]{0,1:T(4,128)} %param.8) | copy-start | bytes 12292
  16.6 26.8 %copy-start.1 = (f32[16,64,256]{2,1,0:T(8,128)S(1)}, f32[16,64,256]{2,1,0:T(8,128)}, u32[]{:S(2)}) copy-start(f32[16,64,256]{2,1,0:T(8,128)} %param.13) | copy-start | bytes 3145732
  16.6 26.9 %copy-start.2 = (f32[16,64,256]{2,1,0:T(8,128)S(1)}, f32[16,64,256]{2,1,0:T(8,128)}, u32[]{:S(2)}) copy-start(f32[16,64,256]{2,1,0:T(8,128)} %param.11) | copy-start | bytes 3145732
  16.6 26.9 %copy-start.3 = (f32[16,64,256]{2,1,0:T(8,128)S(1)}, f32[16,64,256]{2,1,0:T(8,128)}, u32[]{:S(2)}) copy-start(f32[16,64,256]{2,1,0:T(8,128)} %param.12) | copy-start | bytes 3145732
  16.6 26.9 %copy-start.9 = (f32[64]{0:T(128)S(1)}, f32[64]{0:T(128)}, u32[]{:S(2)}) copy-start(f32[64]{0:T(128)} %param.10) | copy-start | bytes 772
  43.4 168.3 %all-gather.7.cloned.1.call-start = ((), (), s32[]{:S(2)}) async-start(), calls=%async_computation.5 | async-start | bytes 5898240 | tf_op jit(solution)/shard_map/all_gather | solution.py:111
  164.1 5.3 %copy-start.6 = (bf16[1,2,1024,256]{3,2,0,1:T(8,128)(2,1)}, bf16[1,2,1024,256]{3,2,0,1:T(8,128)(2,1)S(1)}, u32[]{:S(2)}) copy-start(bf16[1,2,1024,256]{3,2,0,1:T(8,128)(2,1)S(1)} %get-tuple-element.6) | copy-start | bytes 3145732
  164.1 5.3 %copy-start.5 = (bf16[1,2,1024,256]{3,2,0,1:T(8,128)(2,1)}, bf16[1,2,1024,256]{3,2,0,1:T(8,128)(2,1)S(1)}, u32[]{:S(2)}) copy-start(bf16[1,2,1024,256]{3,2,0,1:T(8,128)(2,1)S(1)} %get-tuple-element.5) | copy-start | bytes 3145732
  164.1 47.6 %copy-start.4 = (bf16[1,2,1024,256]{3,2,0,1:T(8,128)(2,1)}, bf16[1,2,1024,256]{3,2,0,1:T(8,128)(2,1)S(1)}, u32[]{:S(2)}) copy-start(bf16[1,2,1024,256]{3,2,0,1:T(8,128)(2,1)S(1)} %get-tuple-element.4) | copy-start | bytes 3145732
  164.1 5.2 %copy-start.10 = (bf16[16,1,80,2048]{3,2,0,1:T(8,128)(2,1)S(1)}, bf16[16,1,80,2048]{3,2,0,1:T(8,128)(2,1)}, u32[]{:S(2)}) copy-start(bf16[16,1,80,2048]{3,2,0,1:T(8,128)(2,1)} %all-gather.5.cloned.1.call-done) | copy-start | bytes 15728644
  211.7 12.7 %copy-start.8 = (f32[256,4]{0,1:T(4,128)S(1)}, f32[256,4]{0,1:T(4,128)}, u32[]{:S(2)}) copy-start(f32[256,4]{0,1:T(4,128)} %param.9) | copy-start | bytes 12292
  216.6 25.7 %all-to-all-start.3 = ((bf16[1,16,80,256]{3,2,0,1:T(8,128)(2,1)}), bf16[1,16,80,256]{3,2,0,1:T(8,128)(2,1)S(1)}, u32[]{:S(2)}, u32[]{:S(2)}) async-start(bf16[1,16,80,256]{3,2,0,1:T(8,128)(2,1)} %fusion.21), calls=%async_computation.3 | async-start | bytes 1310720 | tf_op jit(solution)/shard_map/all_to_all | solution.py:116
Sparse Core Ops, SparseCore 0:
  43.5 41.8 all-gather.4
  172.2 39.4 all-gather.6
where the time goes:
time: 250 us
  blocking collectives  146 us (58%)
  waiting for transfers between devices  53.2 us (21%)
  matrix products  17.6 us (7%)
  between operations  14.4 us (6%)
  other arithmetic  8.79 us (4%)
  starting transfers between devices  7.83 us (3%)
    all_to_all x1, blocking collectives, from_everyone(): lax.all_to_all(jnp.broadcast_to(array[None], (devices, *array.shape)), ax...  77.5 us
    all_to_all x1, blocking collectives, sent_together(): lax.all_to_all(both, axis, split_axis=split_dim, concat_axis=concat_dim,...  41.9 us
    all_gather x1, waiting for transfers between devices, local(): lax.all_gather(hidden, 'tp', axis=3, tiled=True)  39.6 us
    all_to_all x1, blocking collectives, local(): lax.all_to_all(outgoing, 'fs', split_axis=0, concat_axis=1, tiled=True)  26.7 us
    all_to_all x1, waiting for transfers between devices, local(): lax.all_to_all(results, 'fs', split_axis=1, concat_axis=0, tiled=True)  13.5 us
    all_to_all x1, starting transfers between devices, local(): lax.all_to_all(results, 'fs', split_axis=1, concat_axis=0, tiled=True)  7.74 us
    dot_general x1, matrix products, local(): jnp.einsum('egnd,edf->egnf', portion, served_gate, preferred_element_type...  5.17 us
  transfers between devices with their start and end apart: 3, of which 2 were waited for; matrix products, arithmetic and copies ran while one was open for 2% of the time, Pallas kernels for 0%

commit v1 on v0

--- a/solution.py
+++ b/solution.py
@@ -108,7 +108,9 @@
     hidden = activate(gate_pre, up_pre)
     summed = jnp.einsum(
         "egnf,efd->egnd",
-        lax.all_gather(hidden, "tp", axis=3, tiled=True),
+        jnp.concatenate(
+            lax.all_to_all(jnp.stack([hidden] * lax.axis_size("tp")), "tp", 0, 0), axis=3
+        ),
         served_down,
         preferred_element_type=jnp.float32,
     )

time: 250 us -> 287 us (1.15)
  blocking collectives: 146 us -> 211 us
  waiting for transfers between devices: 53.2 us -> 12.7 us
  local copies, waits for them, and re-layouts: 2.3 us -> 17 us
    all_to_all x0 -> x1, blocking collectives: none -> 65 us  [local(): lax.all_to_all(jnp.stack([hidden] * lax.axis_size('tp')), 'tp', 0, 0)]
    all_gather x1 -> x0, waiting for transfers between devices: 39.6 us -> none  [local(): lax.all_gather(hidden, 'tp', axis=3, tiled=True)]
    another operation x2 -> x4, local copies, waits for them, and re-layouts: 0.08 us -> 9.42 us
    reshape x0 -> x1, local copies, waits for them, and re-layouts: none -> 5.37 us  [local(): jnp.concatenate(lax.all_to_all(jnp.stack([hidden] * lax.axis_size('tp')),...]
  transfers between devices with their start and end apart: 3 -> 2, of which waited for: 2 -> 1; matrix products, arithmetic and copies ran while one was open for 2% -> 2% of each run, Pallas kernels for 0% -> 0%
where the time goes in v1:
time: 287 us; the launch traced here: 286 us
  blocking collectives  211 us (74%)
  local copies, waits for them, and re-layouts  17 us (6%)
  matrix products  16.7 us (6%)
  between operations  14.4 us (5%)
  waiting for transfers between devices  12.7 us (4%)
  other arithmetic  8.79 us (3%)
  starting transfers between devices  5.64 us (2%)
    all_to_all x1, blocking collectives, from_everyone(): lax.all_to_all(jnp.broadcast_to(array[None], (devices, *array.shape)), ax...  77.5 us
    all_to_all x1, blocking collectives, local(): lax.all_to_all(jnp.stack([hidden] * lax.axis_size('tp')), 'tp', 0, 0)  65 us
    all_to_all x1, blocking collectives, sent_together(): lax.all_to_all(both, axis, split_axis=split_dim, concat_axis=concat_dim,...  41.9 us
    all_to_all x1, blocking collectives, local(): lax.all_to_all(outgoing, 'fs', split_axis=0, concat_axis=1, tiled=True)  26.7 us
    all_to_all x1, waiting for transfers between devices, local(): lax.all_to_all(results, 'fs', split_axis=1, concat_axis=0, tiled=True)  12.7 us
    another operation x3, local copies, waits for them, and re-layouts  8.99 us
  transfers between devices with their start and end apart: 2, of which 1 were waited for; matrix products, arithmetic and copies ran while one was open for 2% of the time, Pallas kernels for 0%

profile of v1, /device:TPU:32, one launch (start us, length us, event | category | flops | bytes accessed | tf_op | source)
XLA Modules:
  0.0 286.3 jit_solution(1729131744597431133)
XLA Ops:
  7.2 0.0 all-gather.3.cloned.1.call-start
  7.2 0.8 copy.41
  8.0 0.1 eq.44
  8.2 0.1 eq.40
  8.3 0.0 copy-start
  8.3 1.5 convert_element_type.62
  9.8 0.0 copy-done
  9.9 0.0 copy-start.7
  9.9 0.3 multiply_reduce_fusion
  10.2 4.5 %reduce-window.6 = s32[16,8,128]{2,1,0:T(8,128)S(1)} reduce-window(s32[16,8,128]{2,1,0:T(8,128)S(1)} %fusion.29, s32[]{:T(128)} %constant.14.clone.1), window={size=1x1x128 pad=0_0x0_0x127_0}, to_apply=%region_1.0 | reduce-window | flops 2080768 | bytes 131076 | tf_op jit(solution)/shard_map/reduce-window
  14.7 0.1 slice.11
  14.8 0.1 copy.43
  14.9 0.1 copy.44
  15.0 0.1 broadcast_add_fusion
  15.1 0.1 reduce_sum.40
  15.3 0.1 copy.45
  15.3 0.0 copy-done.7
  15.4 0.8 convert_reduce_fusion
  16.2 0.4 convolution_convert_fusion
  16.6 0.0 copy-start.1
  16.6 0.0 copy-start.2
  16.6 0.0 copy-start.3
  16.6 0.0 copy-start.9
  16.7 26.7 %all_to_all.43 = bf16[16,1,80,256]{3,2,1,0:T(8,128)(2,1)} all-to-all(bf16[16,1,80,256]{3,2,1,0:T(8,128)(2,1)S(1)} %bitcast.74), channel_id=1, replica_groups=mesh['gr'=2,'fs'=16,'tp'=8] {'fs'}, dimensions={0} | all-to-all | bytes 1310720 | tf_op jit(solution)/shard_map/all_to_all | solution.py:99
  43.4 0.0 all-gather.3.cloned.1.call-update
  43.4 0.0 copy-done.1
  43.4 0.1 convert_element_type.55
  43.5 0.0 copy-done.2
  43.5 0.0 copy-done.3
  43.5 0.0 copy-done.9
  43.5 0.3 multiply_convert_fusion.1
  43.8 0.1 pad_maximum_fusion
  43.9 41.9 %all_to_all.44 = bf16[16,64,768]{2,1,0:T(8,128)(2,1)S(1)} all-to-all(bf16[16,64,768]{2,1,0:T(8,128)(2,1)S(1)} %pad_maximum_fusion), channel_id=1, replica_groups=mesh['gr'=2,'fs'=16,'tp'=8] {'fs'}, dimensions={0} | all-to-all | bytes 3145728 | tf_op jit(solution)/shard_map/all_to_all | solution.py:21
  85.8 0.1 fusion.33
  85.9 0.2 pad_maximum_fusion.1
  86.1 0.2 broadcast_in_dim.2
  86.3 77.5 %all_to_all.45 = bf16[2,3,1024,256]{3,2,1,0:T(8,128)(2,1)S(1)} all-to-all(bf16[2,3,1024,256]{3,2,1,0:T(8,128)(2,1)S(1)} %broadcast_in_dim.2), channel_id=1, replica_groups=mesh['gr'=2,'fs'=16,'tp'=8] {'gr'}, dimensions={0} | all-to-all | bytes 6291456 | tf_op jit(solution)/shard_map/all_to_all | solution.py:36
  163.8 0.2 fusion.32
  164.0 0.0 copy-start.6
  164.0 0.0 copy-start.5
  164.0 0.0 copy-start.4
  164.1 0.0 all-gather.3.cloned.1.call-done
  164.1 0.0 copy-start.10
  164.1 5.2 %fusion.9 = f32[16,80,256]{2,1,0:T(8,128)S(1)} fusion(bf16[2048,256,1]{1,0,2:T(8,128)(2,1)S(1)} %bitcast.80, bf16[16,1,80,2048]{3,2,0,1:T(8,128)(2,1)} %all-gather.3.cloned.1.call-done), kind=kOutput, calls=%fused_computation.13 | convolution fusion | flops 1342504960 | bytes 7602176 | tf_op jit(solution)/shard_map/egnd,edf->egnf/dot_general | solution.py:104
  169.3 0.0 copy-done.6
  169.3 0.0 copy-done.5
  169.3 0.0 copy-done.10
  169.3 1.8 fusion.18
  171.1 0.4 stack.2
  171.5 65.0 %all_to_all.46 = bf16[8,1,16,80,256]{4,3,2,1,0:T(8,128)(2,1)S(1)} all-to-all(bf16[8,1,16,80,256]{4,3,2,1,0:T(8,128)(2,1)S(1)} %stack.2), channel_id=1, replica_groups=mesh['gr'=2,'fs'=16,'tp'=8] {'tp'}, dimensions={0} | all-to-all | bytes 10485760 | tf_op jit(solution)/shard_map/all_to_all | solution.py:112
  236.6 5.4 %copy.48 = bf16[1,16,80,8,256]{4,3,2,1,0:T(8,128)(2,1)} copy(bf16[1,16,80,8,256]{4,2,1,0,3:T(8,128)(2,1)S(1)} %bitcast.71) | data formatting | bytes 10485760 | tf_op jit(solution)/shard_map/reshape | solution.py:111
  241.9 8.9 %reshape.130 = bf16[16,80,2048]{2,1,0:T(8,128)(2,1)} reshape(bf16[1,16,80,8,256]{4,3,2,1,0:T(8,128)(2,1)} %copy.48) | data formatting | bytes 10485760 | tf_op jit(solution)/shard_map/reshape.29
  250.8 0.0 copy-done.4
  250.8 0.0 copy-start.8
  250.8 4.9 %fusion.21 = bf16[1,16,80,256]{3,2,0,1:T(8,128)(2,1)} fusion(bf16[16,80,2048]{2,1,0:T(8,128)(2,1)} %reshape.130, bf16[2048,256,1]{1,0,2:T(8,128)(2,1)S(1)} %bitcast.76), kind=kOutput, calls=%fused_computation.19 | convolution fusion | flops 1342504960 | bytes 6946816 | tf_op jit(solution)/shard_map/egnf,efd->egnd/dot_general | solution.py:109
  255.7 5.6 %all-to-all-start.4 = ((bf16[1,16,80,256]{3,2,0,1:T(8,128)(2,1)}), bf16[1,16,80,256]{3,2,0,1:T(8,128)(2,1)S(1)}, u32[]{:S(2)}, u32[]{:S(2)}) async-start(bf16[1,16,80,256]{3,2,0,1:T(8,128)(2,1)} %fusion.21), calls=%async_computation.4 | async-start | bytes 1310720 | tf_op jit(solution)/shard_map/all_to_all | solution.py:118
  261.3 0.0 copy-done.8
  261.4 0.2 copy.50
  261.6 0.8 iota_compare_fusion
  262.4 3.4 %fusion.4 = bf16[256,1,1280]{2,1,0:T(2,128)(2,1)S(1)} fusion(bf16[256,4,1]{1,2,0:T(2,128)(2,1)S(1)} %copy.50, pred[256,4,1280]{2,0,1:T(32,128)(4,1)S(1)} %iota_compare_fusion), kind=kOutput, calls=%fused_computation.6 | convolution fusion | flops 2621440 | bytes 1968128 | tf_op jit(solution)/shard_map/tk,tkc->tc/dot_general | solution.py:66
  265.8 12.7 %all-to-all-done.4 = bf16[1,16,80,256]{3,2,0,1:T(8,128)(2,1)S(1)} async-done(((bf16[1,16,80,256]{3,2,0,1:T(8,128)(2,1)}), bf16[1,16,80,256]{3,2,0,1:T(8,128)(2,1)S(1)}, u32[]{:S(2)}, u32[]{:S(2)}) %all-to-all-start.4) | async-done | bytes 655392 | tf_op jit(solution)/shard_map/all_to_all | solution.py:118
  278.5 1.0 convolution_convert_fusion.2
  (8 shorter events, 0.1 us)
Async XLA Ops:
  7.2 156.9 %all-gather.3.cloned.1.call-start = ((), (), s32[]{:S(2)}) async-start(), calls=%async_computation.5 | async-start | bytes 5898240 | tf_op jit(solution)/shard_map/all_gather | solution.py:98
  8.3 1.6 copy-start
  9.9 5.5 %copy-start.7 = (s32[256,4]{0,1:T(4,128)S(1)}, s32[256,4]{0,1:T(4,128)}, u32[]{:S(2)}) copy-start(s32[256,4]{0,1:T(4,128)} %param.8) | copy-start | bytes 12292
  16.6 26.8 %copy-start.1 = (f32[16,64,256]{2,1,0:T(8,128)S(1)}, f32[16,64,256]{2,1,0:T(8,128)}, u32[]{:S(2)}) copy-start(f32[16,64,256]{2,1,0:T(8,128)} %param.13) | copy-start | bytes 3145732
  16.6 26.9 %copy-start.2 = (f32[16,64,256]{2,1,0:T(8,128)S(1)}, f32[16,64,256]{2,1,0:T(8,128)}, u32[]{:S(2)}) copy-start(f32[16,64,256]{2,1,0:T(8,128)} %param.11) | copy-start | bytes 3145732
  16.6 26.9 %copy-start.3 = (f32[16,64,256]{2,1,0:T(8,128)S(1)}, f32[16,64,256]{2,1,0:T(8,128)}, u32[]{:S(2)}) copy-start(f32[16,64,256]{2,1,0:T(8,128)} %param.12) | copy-start | bytes 3145732
  16.6 26.8 %copy-start.9 = (f32[64]{0:T(128)S(1)}, f32[64]{0:T(128)}, u32[]{:S(2)}) copy-start(f32[64]{0:T(128)} %param.10) | copy-start | bytes 772
  164.0 5.3 %copy-start.6 = (bf16[1,2,1024,256]{3,2,0,1:T(8,128)(2,1)}, bf16[1,2,1024,256]{3,2,0,1:T(8,128)(2,1)S(1)}, u32[]{:S(2)}) copy-start(bf16[1,2,1024,256]{3,2,0,1:T(8,128)(2,1)S(1)} %get-tuple-element.6) | copy-start | bytes 3145732
  164.0 5.3 %copy-start.5 = (bf16[1,2,1024,256]{3,2,0,1:T(8,128)(2,1)}, bf16[1,2,1024,256]{3,2,0,1:T(8,128)(2,1)S(1)}, u32[]{:S(2)}) copy-start(bf16[1,2,1024,256]{3,2,0,1:T(8,128)(2,1)S(1)} %get-tuple-element.5) | copy-start | bytes 3145732
  164.0 86.8 %copy-start.4 = (bf16[1,2,1024,256]{3,2,0,1:T(8,128)(2,1)}, bf16[1,2,1024,256]{3,2,0,1:T(8,128)(2,1)S(1)}, u32[]{:S(2)}) copy-start(bf16[1,2,1024,256]{3,2,0,1:T(8,128)(2,1)S(1)} %get-tuple-element.4) | copy-start | bytes 3145732
  164.1 5.2 %copy-start.10 = (bf16[16,1,80,2048]{3,2,0,1:T(8,128)(2,1)S(1)}, bf16[16,1,80,2048]{3,2,0,1:T(8,128)(2,1)}, u32[]{:S(2)}) copy-start(bf16[16,1,80,2048]{3,2,0,1:T(8,128)(2,1)} %all-gather.3.cloned.1.call-done) | copy-start | bytes 15728644
  250.8 10.5 %copy-start.8 = (f32[256,4]{0,1:T(4,128)S(1)}, f32[256,4]{0,1:T(4,128)}, u32[]{:S(2)}) copy-start(f32[256,4]{0,1:T(4,128)} %param.9) | copy-start | bytes 12292
  255.7 22.7 %all-to-all-start.4 = ((bf16[1,16,80,256]{3,2,0,1:T(8,128)(2,1)}), bf16[1,16,80,256]{3,2,0,1:T(8,128)(2,1)S(1)}, u32[]{:S(2)}, u32[]{:S(2)}) async-start(bf16[1,16,80,256]{3,2,0,1:T(8,128)(2,1)} %fusion.21), calls=%async_computation.4 | async-start | bytes 1310720 | tf_op jit(solution)/shard_map/all_to_all | solution.py:118
Sparse Core Ops, SparseCore 0:
  43.5 41.8 all-gather.2
